TPU v7x, 256 devices: a whole 4x4x8 slice. The times are simulated.
256 devices in a mesh: ep: 64 (over z, x, core), tp: 4 (over y).
Axes of the slice: x: 4, y: 4, z: 8, core: 2. Of those that a mesh axis runs over, the one named last changes fastest.
Arguments:
- queries: bfloat16 [16384, 8, 128], P('ep', 'tp'), may hold values from -256 to 256
- keys: bfloat16 [16384, 4, 128], P('ep', 'tp'), may hold values from -8 to 8
- values: bfloat16 [16384, 4, 128], P('ep', 'tp'), may hold values from -6 to 6
- attn_lambda: float32 [8], P('tp'), may hold values from 0.3 to 0.8
- head_gain: float32 [128], replicated, may hold values from 0.1 to 1.9
- w_out: bfloat16 [1024, 2048], replicated, may hold values from -0.1875 to 0.1875
- moe_rows: bfloat16 [32768, 2048], P('ep'), may hold values from -6 to 6
- moe_gain: float32 [2048], replicated, may hold values from 0.1 to 1.9
- routes: int32 [32768, 2], P('ep'), may hold values from 0 to 63, all different within a row; in each aligned block of 128 rows (0 to 127, 128 to 255, ...) at most 8 rows name the same one
- route_weights: float32 [32768, 2], P('ep'), may hold values from 0.1 to 1
- w_gate: bfloat16 [64, 2048, 1024], P('ep', None, 'tp'), may hold values from -0.125 to 0.125
- w_up: bfloat16 [64, 2048, 1024], P('ep', None, 'tp'), may hold values from -0.125 to 0.125
- w_down: bfloat16 [64, 1024, 2048], P('ep', 'tp'), may hold values from -0.1875 to 0.1875
Outputs:
- mixer_out: bfloat16 [16384, 2048], P(('ep', 'tp'))
- moe_out: bfloat16 [32768, 2048], P(('ep', 'tp'))
Inputs may be any that keep to these rules, and one draw needn't show every extreme that they name: `routes`: each row names 2 different experts. In each aligned block of 128 rows (the rows of moe_out that one device holds) no expert is named by more than 8 rows, a bound that some block reaches.
All inputs are finite; a program needn't handle non-finite values.
Results may differ from a plain program's by a relative error of at most 0.011.
Values may be sent and summed in bfloat16 or wider, within the bound.
No kernel may reach another device: no remote copies, remote signals or barrier semaphores. Data moves between devices by JAX's collectives and lax.ppermute only.
A program may use at most 128 MiB of HBM per device.

v0:
```python
import jax
import jax.numpy as jnp
from jax import lax
from jax.sharding import PartitionSpec as P

EPSILON = 1e-06
MASKED = -1e30


def split_up(x, dim, size):
    before, after = (x.shape[:dim], x.shape[dim + 1 :])
    return jnp.moveaxis(x.reshape(*before, size, -1, *after), dim, 0)


def sum_at_owner(x, axis, dim):
    size = lax.axis_size(axis)
    tiles = lax.all_to_all(split_up(x, dim, size), axis, 0, 0, tiled=True)
    return jnp.sum(tiles.astype(jnp.float32), axis=0)


def joined_along(tiles, dim):
    tiles = jnp.moveaxis(tiles, 0, dim)
    lengths = tiles.shape
    return tiles.reshape(*lengths[:dim], lengths[dim] * lengths[dim + 1], *lengths[dim + 2 :])


def piecewise(x, axis, dim, work, out_dim):
    span = x.shape[dim]
    pieces = jnp.split(x, 2, axis=dim) if span % 2 == 0 else [x]
    first = jnp.arange(lax.axis_size(axis)) * span
    tiles = [lax.all_gather(section, axis) for section in pieces]
    made = [jax.vmap(work)(b, first + k * (span // len(pieces))) for k, b in enumerate(tiles)]
    return joined_along(jnp.concatenate(made, axis=out_dim + 1), out_dim)


def rms_scaled(values_f, gain):
    mean_sq = jnp.mean(values_f * values_f, axis=-1, keepdims=True)
    return values_f * lax.rsqrt(mean_sq + EPSILON) * gain


def slot_numbers(block_routes, experts):
    flat_ids = block_routes.reshape(-1)
    matches = (flat_ids[:, None] == lax.iota(jnp.int32, experts)[None, :]).astype(jnp.int32)
    earlier = jnp.cumsum(matches, axis=0) - matches
    return jnp.sum(earlier * matches, axis=1).reshape(block_routes.shape)


def fill_slots(block_rows, block_routes, experts, capacity):
    slot_ids = slot_numbers(block_routes, experts)
    model_width = block_rows.shape[1]
    copies = jnp.broadcast_to(block_rows[:, None, :], block_routes.shape + (model_width,))
    blank_slots = jnp.zeros((experts, capacity, model_width), block_rows.dtype)
    return (blank_slots.at[block_routes, slot_ids].set(copies), slot_ids)


def local(
    queries,
    keys,
    values,
    attn_lambda,
    head_gain,
    w_out,
    moe_rows,
    moe_gain,
    routes,
    route_weights,
    w_gate,
    w_up,
    w_down,
):
    positions = queries.shape[0]
    q_heads = queries.shape[1]
    kv_heads = keys.shape[1]
    head_dim = queries.shape[2] // 2
    value_dim = values.shape[2]
    per_key = q_heads // kv_heads
    first_pos = lax.axis_index("ep") * positions
    query_pos = first_pos + lax.iota(jnp.int32, positions)
    last_pos = first_pos + positions - 1
    query_view = queries.reshape(positions, kv_heads, per_key, 2, head_dim)
    inv_scale = head_dim ** (-0.5)
    start_max = jnp.full((positions, kv_heads, per_key, 2), MASKED, jnp.float32)
    start_total = jnp.zeros((positions, kv_heads, per_key, 2), jnp.float32)
    start_acc = jnp.zeros((positions, kv_heads, per_key, 2, value_dim), jnp.float32)
    carry = (start_max, start_total, start_acc)
    key_piece = lax.all_gather(keys, "ep", axis=0, tiled=True)
    value_piece = lax.all_gather(values, "ep", axis=0, tiled=True)
    shard_count = key_piece.shape[0] // positions
    together = 1
    for candidate in (2, 3, 4):
        if shard_count % candidate == 0:
            together = candidate
    block_len = together * positions
    blocks = shard_count // together
    key_blocks = key_piece.reshape(blocks, block_len, kv_heads, 2, head_dim)
    value_blocks = value_piece.reshape(blocks, block_len, kv_heads, value_dim)
    block_starts = block_len * lax.iota(jnp.int32, blocks)

    def visit(running, inputs):
        key_blk, value_blk, block_start = inputs

        def update(current):
            run_max, run_total, run_acc = current
            key_pos = block_start + lax.iota(jnp.int32, block_len)
            scores = (
                jnp.einsum(
                    "qkgmd,pkmd->qkgmp", query_view, key_blk, preferred_element_type=jnp.float32
                )
                * inv_scale
            )
            allowed = key_pos[None, :] <= query_pos[:, None]
            scores = jnp.where(allowed[:, None, None, None, :], scores, MASKED)
            new_max = jnp.maximum(run_max, jnp.max(scores, axis=-1))
            shrink = jnp.exp(run_max - new_max)
            weights = jnp.exp(scores - new_max[..., None])
            run_total = run_total * shrink + jnp.sum(weights, axis=-1)
            run_acc = run_acc * shrink[..., None] + jnp.einsum(
                "qkgmp,pkv->qkgmv",
                weights.astype(jnp.bfloat16),
                value_blk,
                preferred_element_type=jnp.float32,
            )
            return (new_max, run_total, run_acc)

        def keep(current):
            return current

        return (lax.cond(block_start <= last_pos, update, keep, running), None)

    carry, unused = lax.scan(visit, carry, (key_blocks, value_blocks, block_starts))
    run_max, run_total, run_acc = carry
    ratios = run_acc / run_total[..., None]
    lambda_view = attn_lambda.reshape(1, kv_heads, per_key, 1)
    head_out = ratios[:, :, :, 0] - lambda_view * ratios[:, :, :, 1]
    attn_rows = (
        rms_scaled(head_out, head_gain).astype(jnp.bfloat16).reshape(positions, q_heads * value_dim)
    )
    tp_count = lax.axis_size("tp")
    tp_id = lax.axis_index("tp")
    head_width = q_heads * value_dim
    w_local = lax.dynamic_slice_in_dim(w_out, tp_id * head_width, head_width, 0)
    mixer_out = sum_at_owner(
        jnp.dot(attn_rows, w_local, preferred_element_type=jnp.float32).astype(jnp.bfloat16),
        "tp",
        0,
    ).astype(jnp.bfloat16)
    experts = lax.axis_size("ep")
    dev_rows = moe_rows.shape[0] // tp_count
    top_count = routes.shape[1]
    capacity = max(2, 2 * dev_rows * top_count // experts)
    model_width = moe_rows.shape[1]
    hidden_units = w_gate.shape[2]
    own_routes = lax.dynamic_slice_in_dim(routes, tp_id * dev_rows, dev_rows, 0)
    own_weights = lax.dynamic_slice_in_dim(route_weights, tp_id * dev_rows, dev_rows, 0)

    def expert_hidden(slot_rows):
        flat_rows = slot_rows.reshape(-1, model_width)
        gate_out = jnp.dot(flat_rows, w_gate[0], preferred_element_type=jnp.float32)
        up_out = jnp.dot(flat_rows, w_up[0], preferred_element_type=jnp.float32)
        return (
            (jax.nn.silu(gate_out) * up_out)
            .astype(jnp.bfloat16)
            .reshape(slot_rows.shape[:-1] + (hidden_units,))
        )

    own_rows = rms_scaled(
        lax.dynamic_slice_in_dim(moe_rows, tp_id * dev_rows, dev_rows, 0).astype(jnp.float32),
        moe_gain,
    ).astype(jnp.bfloat16)
    outgoing, own_slots = fill_slots(own_rows, own_routes, experts, capacity)
    arrived = lax.all_to_all(outgoing, "ep", split_axis=0, concat_axis=0, tiled=True)

    def hidden_piece(slot_rows, begin_row):
        return expert_hidden(slot_rows)

    hidden = piecewise(arrived[None], "tp", 0, hidden_piece, 0)
    all_units = lax.all_to_all(hidden, "tp", split_axis=0, concat_axis=3, tiled=True)
    down_whole = lax.all_gather(w_down[0], "tp", axis=0, tiled=True)
    flat_units = all_units.reshape(-1, tp_count * hidden_units)
    summed_f = jnp.zeros((flat_units.shape[0], model_width), jnp.float32)
    for group in range(tp_count):
        unit_block = flat_units[:, group * hidden_units : (group + 1) * hidden_units]
        weight_block = down_whole[group * hidden_units : (group + 1) * hidden_units]
        group_part = jnp.dot(unit_block, weight_block, preferred_element_type=jnp.float32).astype(
            jnp.bfloat16
        )
        summed_f = summed_f + group_part.astype(jnp.float32)
    summed = summed_f.astype(jnp.bfloat16).reshape(all_units.shape[:-1] + (model_width,))
    returned = lax.all_to_all(summed, "ep", split_axis=1, concat_axis=1, tiled=True)[0]
    picked = returned[own_routes, own_slots]
    moe_out = jnp.sum(own_weights[..., None] * picked.astype(jnp.float32), axis=1).astype(
        jnp.bfloat16
    )
    return (mixer_out, moe_out)


def solution(mesh):
    return jax.shard_map(
        local,
        mesh=mesh,
        in_specs=(
            P("ep", "tp", None),
            P("ep", "tp", None),
            P("ep", "tp", None),
            P("tp"),
            P(),
            P(),
            P("ep", None),
            P(),
            P("ep", None),
            P("ep", None),
            P("ep", None, "tp"),
            P("ep", None, "tp"),
            P("ep", "tp", None),
        ),
        out_specs=(P(("ep", "tp"), None), P(("ep", "tp"), None)),
        check_vma=False,
    )
```

profile of v0, /device:TPU:2, one launch (start us, length us, event | category | flops | bytes accessed | tf_op | source)
XLA Modules:
  0.0 434.8 jit_solution(10305571413842020620)
XLA Ops:
  11.1 1.2 fusion.25
  12.3 1.3 fusion.27
  14.2 1.2 reshape.247
  15.7 33.0 %scatter_fusion = bf16[64,8,2048]{2,1,0:T(8,128)(2,1)S(1)} fusion(bf16[64,8,2048]{2,1,0:T(8,128)(2,1)S(1)} %broadcast_in_dim.36, s32[256]{0:T(256)S(1)} %reshape.245, bf16[256,2048]{1,0:T(8,128)(2,1)} %reshape.247), kind=kCustom, calls=%fused_computation.1 | custom fusion | bytes 3147776 | tf_op jit(solution)/shard_map/scatter | solution.py:53
  48.8 73.1 %all_to_all.30 = bf16[64,8,2048]{2,1,0:T(8,128)(2,1)} all-to-all(bf16[64,8,2048]{2,1,0:T(8,128)(2,1)S(1)} %scatter_fusion), channel_id=1, replica_groups=mesh['ep'=64,'tp'=4] {'ep'}, dimensions={0} | all-to-all | bytes 4194304 | tf_op jit(solution)/shard_map/all_to_all | solution.py:171
  122.7 14.7 %reshape.263 = bf16[16,1024,1,2,64]{4,3,1,0,2:T(2,128)(2,1)} reshape(bf16[16384,1,128]{2,0,1:T(8,128)(2,1)} %all-gather.7.cloned.1.call-done) | data formatting | bytes 8388608 | tf_op jit(solution)/shard_map/reshape | solution.py:95
  137.4 20.2 %copy.37 = bf16[16,1024,1,2,64]{1,4,3,2,0:T(8,128)(2,1)} copy(bf16[16,1024,1,2,64]{4,3,1,0,2:T(2,128)(2,1)} %reshape.263) | data formatting | bytes 8388608
  157.6 29.6 %all-gather.9.cloned.1.call-done = bf16[16384,1,128]{2,0,1:T(8,128)(2,1)} async-done(((bf16[256,1,128]{2,0,1:T(8,128)(2,1)}), bf16[16384,1,128]{2,0,1:T(8,128)(2,1)}) %all-gather.9.cloned.1.call-update) | async-done | bytes 4194320 | tf_op jit(solution)/shard_map/all_gather | solution.py:87
  187.2 6.4 %copy.39 = bf16[16,1024,1,128]{1,3,2,0:T(8,128)(2,1)} copy(bf16[16,1024,1,128]{3,1,0,2:T(8,128)(2,1)} %bitcast.160) | data formatting | bytes 8388608
  193.6 23.8 %while.15 = (s32[]{:T(128)}, f32[256,1,2,2]{0,2,3,1:T(2,128)S(1)}, f32[256,1,2,2]{0,2,3,1:T(2,128)S(1)}, f32[256,1,2,2,128]{0,4,3,2,1:T(8,128)S(1)}, s32[16]{0:T...) while((s32[]{:T(128)}, f32[256,1,2,2]{0,2,3,1:T(2,128)S(1)}, ...), condition=%wide.region_5.6_spmd.clone, body=%wide.region_0.5_spmd.clone.sunk | while | flops 411570432 | bytes 15156511 | solution.py:130
  194.8 5.2 %conditional.3 = ((f32[256,1,2,2]{0,2,3,1:T(2,128)S(1)}, f32[256,1,2,2]{0,2,3,1:T(2,128)S(1)}, f32[256,1,2,2,128]{0,4,3,2,1:T(8,128)S(1)})) conditional(s32[]{:T(128)} %convert_element_type.131, (f32[256,1,2,2]{0,2,3,1:T(2,128)S(1)}, f32[256,1,2,2]{0,2,3,1:T(2,128)S(1)}, f32[256,1,2,2,128]{0,4,3,2,1:T(8,128)S(1)}) %tuple.48, (s32[]{:T(128)}, ...), branch_computations={%region_1.1_spmd, %region_2.4_spmd} | conditional | flops 411570432 | bytes 15155240 | solution.py:128
  195.6 1.8 fusion.4
  198.5 1.5 fusion.11
  217.5 55.6 %all-gather.11.cloned.1.call-done = bf16[256,8,2048]{2,1,0:T(8,128)(2,1)} async-done(((bf16[64,8,2048]{2,1,0:T(8,128)(2,1)}), bf16[256,8,2048]{2,1,0:T(8,128)(2,1)}) %all-gather.11.cloned.1.call-update) | async-done | bytes 8388624 | tf_op jit(solution)/shard_map/all_gather | solution.py:31
  273.1 5.9 %fusion.28 = f32[4,512,256]{2,1,0:T(8,128)S(1)} fusion(bf16[4,512,2048]{2,1,0:T(8,128)(2,1)} %bitcast.170, bf16[1,2048,256]{2,1,0:T(8,128)(2,1)S(1)} %copy-done), kind=kOutput, calls=%fused_computation.47 | convolution fusion | flops 2147483648 | bytes 11534336 | tf_op jit(solution)/shard_map/vmap()/dot_general | solution.py:159
  279.1 3.6 fusion.24
  282.7 4.0 all-to-all-start.2
  287.0 2.8 convolution_convert_fusion.4
  289.8 22.2 %all-to-all-done.2 = bf16[4,64,8,256]{3,2,1,0:T(8,128)(2,1)S(1)} async-done(((bf16[4,64,8,256]{3,2,1,0:T(8,128)(2,1)}), bf16[4,64,8,256]{3,2,1,0:T(8,128)(2,1)S(1)}, u32[]{:S(2)}, u32[]{:S(2)}) %all-to-all-start.2) | async-done | bytes 1048608 | tf_op jit(solution)/shard_map/all_to_all | solution.py:177
  312.0 3.7 all-to-all-start
  315.7 1.4 copy.65
  317.3 29.3 %all-gather.13.cloned.1.call-done = bf16[1,1024,2048]{2,1,0:T(8,128)(2,1)} async-done(((bf16[1,256,2048]{2,1,0:T(8,128)(2,1)}), bf16[1,1024,2048]{2,1,0:T(8,128)(2,1)}) %all-gather.13.cloned.1.call-update) | async-done | bytes 4194320 | tf_op jit(solution)/shard_map/all_gather | solution.py:178
  346.6 2.1 convolution_convert_fusion
  348.7 1.9 convolution_convert_fusion.1
  351.4 2.6 fusion.23
  354.0 1.0 copy-done.2
  355.0 10.6 %all-to-all-start.3 = ((bf16[1,64,8,2048]{3,2,0,1:T(8,128)(2,1)}), bf16[1,64,8,2048]{3,2,0,1:T(8,128)(2,1)S(1)}, u32[]{:S(2)}, u32[]{:S(2)}) async-start(bf16[1,64,8,2048]{3,2,0,1:T(8,128)(2,1)} %fusion.23), calls=%async_computation.3 | async-start | bytes 4194304 | tf_op jit(solution)/shard_map/all_to_all | solution.py:189
  366.5 2.2 reduce_sum.60
  368.7 48.1 %all-to-all-done.3 = bf16[1,64,8,2048]{3,2,0,1:T(8,128)(2,1)S(1)} async-done(((bf16[1,64,8,2048]{3,2,0,1:T(8,128)(2,1)}), bf16[1,64,8,2048]{3,2,0,1:T(8,128)(2,1)S(1)}, u32[]{:S(2)}, u32[]{:S(2)}) %all-to-all-start.3) | async-done | bytes 2097184 | tf_op jit(solution)/shard_map/all_to_all | solution.py:189
  416.8 5.2 %gather_fusion = bf16[256,2048]{1,0:T(8,128)(2,1)} fusion(bf16[64,8,2048]{2,1,0:T(8,128)(2,1)S(1)} %bitcast.159, s32[256]{0:T(256)S(1)} %reshape.239), kind=kCustom, calls=%fused_computation | custom fusion | bytes 2099200 | tf_op jit(solution)/shard_map/gather | solution.py:190
  422.0 2.4 reshape.258
  424.4 3.9 multiply_reduce_fusion
  (114 shorter events, 18.9 us)
Async XLA Ops:
  7.2 266.0 %copy-start = (bf16[1,2048,256]{2,1,0:T(8,128)(2,1)S(1)}, bf16[1,2048,256]{2,1,0:T(8,128)(2,1)}, u32[]{:S(2)}) copy-start(bf16[1,2048,256]{2,1,0:T(8,128)(2,1)} %param.28) | copy-start | bytes 3145732
  7.2 115.6 %all-gather.7.cloned.1.call-start = ((), (), s32[]{:S(2)}) async-start(), calls=%async_computation.4 | async-start | bytes 4259840 | tf_op jit(solution)/shard_map/all_gather | solution.py:86
  7.9 179.3 %all-gather.9.cloned.1.call-start = ((), (), s32[]{:S(2)}) async-start(), calls=%async_computation.5 | async-start | bytes 4259840 | tf_op jit(solution)/shard_map/all_gather | solution.py:87
  8.7 264.5 %all-gather.11.cloned.1.call-start = ((), (), s32[]{:S(2)}) async-start(), calls=%async_computation.6 | async-start | bytes 10485760 | tf_op jit(solution)/shard_map/all_gather | solution.py:31
  48.7 73.8 %copy-start.3 = (bf16[256,2,128]{2,1,0:T(2,128)(2,1)S(1)}, bf16[256,2,128]{2,1,0:T(2,128)(2,1)}, u32[]{:S(2)}) copy-start(bf16[256,2,128]{2,1,0:T(2,128)(2,1)} %param.17) | copy-start | bytes 393220
  48.7 73.9 %copy-start.4 = (f32[2]{0:T(128)S(1)}, f32[2]{0:T(128)}, u32[]{:S(2)}) copy-start(f32[2]{0:T(128)} %param.20) | copy-start | bytes 28
  48.8 73.9 %copy-start.5 = (f32[128]{0:T(128)S(1)}, f32[128]{0:T(128)}, u32[]{:S(2)}) copy-start(f32[128]{0:T(128)} %param.21) | copy-start | bytes 1540
  121.9 224.7 %all-gather.13.cloned.1.call-start = ((), (), s32[]{:S(2)}) async-start(), calls=%async_computation.7 | async-start | bytes 5242880 | tf_op jit(solution)/shard_map/all_gather | solution.py:178
  273.1 5.9 %copy-start.6 = (bf16[256,8,2048]{2,1,0:T(8,128)(2,1)S(1)}, bf16[256,8,2048]{2,1,0:T(8,128)(2,1)}, u32[]{:S(2)}) copy-start(bf16[256,8,2048]{2,1,0:T(8,128)(2,1)} %all-gather.11.cloned.1.call-done) | copy-start | bytes 25165828
  273.1 6.0 %copy-start.7 = (bf16[1,2048,256]{2,1,0:T(8,128)(2,1)S(1)}, bf16[1,2048,256]{2,1,0:T(8,128)(2,1)}, u32[]{:S(2)}) copy-start(bf16[1,2048,256]{2,1,0:T(8,128)(2,1)} %param.27) | copy-start | bytes 3145732
  282.7 29.3 %all-to-all-start.2 = ((bf16[4,64,8,256]{3,2,1,0:T(8,128)(2,1)}), bf16[4,64,8,256]{3,2,1,0:T(8,128)(2,1)S(1)}, u32[]{:S(2)}, u32[]{:S(2)}) async-start(bf16[4,64,8,256]{3,2,1,0:T(8,128)(2,1)} %fusion.24), calls=%async_computation.2 | async-start | bytes 2097152 | tf_op jit(solution)/shard_map/all_to_all | solution.py:177
  312.0 42.0 %all-to-all-start = ((bf16[4,64,2048]{2,1,0:T(8,128)(2,1)}), bf16[4,64,2048]{2,1,0:T(8,128)(2,1)S(1)}, u32[]{:S(2)}, u32[]{:S(2)}) async-start(bf16[4,64,2048]{2,1,0:T(8,128)(2,1)} %bitcast.26), calls=%async_computation | async-start | bytes 2097152 | tf_op jit(solution)/shard_map/all_to_all | solution.py:17
  346.6 4.0 copy-start.1
  354.0 1.0 copy-start.2
  355.0 61.8 %all-to-all-start.3 = ((bf16[1,64,8,2048]{3,2,0,1:T(8,128)(2,1)}), bf16[1,64,8,2048]{3,2,0,1:T(8,128)(2,1)S(1)}, u32[]{:S(2)}, u32[]{:S(2)}) async-start(bf16[1,64,8,2048]{3,2,0,1:T(8,128)(2,1)} %fusion.23), calls=%async_computation.3 | async-start | bytes 4194304 | tf_op jit(solution)/shard_map/all_to_all | solution.py:189
Sparse Core Ops, SparseCore 0:
  10.8 94.4 all-gather.6
  108.0 79.1 all-gather.8
  189.0 84.0 all-gather.10
  274.8 71.7 all-gather.12
where the time goes:
time: 438 us; the launch traced here: 435 us
  waiting for transfers between devices  187 us (43%)
  local copies, waits for them, and re-layouts  98.3 us (22%)
  blocking collectives  73.1 us (17%)
  matrix products  23 us (5%)
  starting transfers between devices  18.6 us (4%)
  between operations  14.1 us (3%)
  other arithmetic  11.5 us (3%)
  loops' own time  9.72 us (2%)
    all_to_all x1, blocking collectives, local(): lax.all_to_all(outgoing, 'ep', split_axis=0, concat_axis=0, tiled=True)  73.1 us
    all_gather x1, waiting for transfers between devices, piecewise(): tiles = [lax.all_gather(section, axis) for section in pieces]  55.6 us
    all_to_all x1, waiting for transfers between devices, local(): lax.all_to_all(summed, 'ep', split_axis=1, concat_axis=1, tiled=True)[0]  48.1 us
    scatter x1, local copies, waits for them, and re-layouts, fill_slots(): return (blank_slots.at[block_routes, slot_ids].set(copies), slot_ids)  33 us
    all_gather x1, waiting for transfers between devices, local(): value_piece = lax.all_gather(values, 'ep', axis=0, tiled=True)  29.6 us
    all_gather x1, waiting for transfers between devices, local(): down_whole = lax.all_gather(w_down[0], 'tp', axis=0, tiled=True)  29.3 us
    unnamed x22, local copies, waits for them, and re-layouts  28.1 us
    all_to_all x1, waiting for transfers between devices, local(): lax.all_to_all(hidden, 'tp', split_axis=0, concat_axis=3, tiled=True)  22.2 us
  transfers between devices with their start and end apart: 7, of which 5 were waited for; matrix products, arithmetic and copies ran while one was open for 28% of the time, Pallas kernels for 0%

commit v1 on v0

--- a/solution.py
+++ b/solution.py
@@ -83,8 +83,11 @@
     start_total = jnp.zeros((positions, kv_heads, per_key, 2), jnp.float32)
     start_acc = jnp.zeros((positions, kv_heads, per_key, 2, value_dim), jnp.float32)
     carry = (start_max, start_total, start_acc)
-    key_piece = lax.all_gather(keys, "ep", axis=0, tiled=True)
-    value_piece = lax.all_gather(values, "ep", axis=0, tiled=True)
+    key_piece, value_piece = jnp.split(
+        lax.all_gather(jnp.concatenate([keys, values], axis=1), "ep", axis=0, tiled=True),
+        [keys.shape[1]],
+        axis=1,
+    )
     shard_count = key_piece.shape[0] // positions
     together = 1
     for candidate in (2, 3, 4):

time: 438 us -> 410 us (0.936)
  waiting for transfers between devices: 187 us -> 111 us
  starting transfers between devices: 18.6 us -> 45.9 us
  blocking collectives: 73.1 us -> 82.9 us
  local copies, waits for them, and re-layouts: 98.3 us -> 105 us
    all_gather x1, waiting for transfers between devices: 55.6 us -> 11.3 us  [piecewise(): tiles = [lax.all_gather(section, axis) for section in pieces]]
    all_gather x2 -> x1, waiting for transfers between devices: 29.6 us -> 0.01 us  [local(): lax.all_gather(jnp.concatenate([keys, values], axis=1), 'ep', axis=0, til...]
    all_to_all x1, starting transfers between devices: 10.6 us -> 37.9 us  [local(): lax.all_to_all(summed, 'ep', split_axis=1, concat_axis=1, tiled=True)[0]]
    all_to_all x1, blocking collectives: 73.1 us -> 82.9 us  [local(): lax.all_to_all(outgoing, 'ep', split_axis=0, concat_axis=0, tiled=True)]
    split x0 -> x1, local copies, waits for them, and re-layouts: none -> 5.8 us  [local(): jnp.split(lax.all_gather(jnp.concatenate([keys, values], axis=1), 'ep', a...]
  transfers between devices with their start and end apart: 7 -> 6, of which waited for: 5 -> 4; matrix products, arithmetic and copies ran while one was open for 28% -> 31% of each run, Pallas kernels for 0% -> 0%
where the time goes in v1:
time: 410 us; the launch traced here: 407 us
  waiting for transfers between devices  111 us (27%)
  local copies, waits for them, and re-layouts  105 us (26%)
  blocking collectives  82.9 us (20%)
  starting transfers between devices  45.9 us (11%)
  matrix products  22.9 us (6%)
  between operations  14.1 us (3%)
  other arithmetic  13.2 us (3%)
  loops' own time  11.1 us (3%)
    all_to_all x1, blocking collectives, local(): lax.all_to_all(outgoing, 'ep', split_axis=0, concat_axis=0, tiled=True)  82.9 us
    all_to_all x1, waiting for transfers between devices, local(): lax.all_to_all(summed, 'ep', split_axis=1, concat_axis=1, tiled=True)[0]  48.1 us
    all_to_all x1, starting transfers between devices, local(): lax.all_to_all(summed, 'ep', split_axis=1, concat_axis=1, tiled=True)[0]  37.9 us
    scatter x1, local copies, waits for them, and re-layouts, fill_slots(): return (blank_slots.at[block_routes, slot_ids].set(copies), slot_ids)  33 us
    all_gather x1, waiting for transfers between devices, local(): down_whole = lax.all_gather(w_down[0], 'tp', axis=0, tiled=True)  29.4 us
    unnamed x22, local copies, waits for them, and re-layouts  28.2 us
    all_to_all x1, waiting for transfers between devices, local(): lax.all_to_all(hidden, 'tp', split_axis=0, concat_axis=3, tiled=True)  22.1 us
    reshape x1, local copies, waits for them, and re-layouts, local(): key_blocks = key_piece.reshape(blocks, block_len, kv_heads, 2, head_dim)  14.8 us
  transfers between devices with their start and end apart: 6, of which 4 were waited for; matrix products, arithmetic and copies ran while one was open for 31% of the time, Pallas kernels for 0%

profile of v1, /device:TPU:2, one launch (start us, length us, event | category | flops | bytes accessed | tf_op | source)
XLA Modules:
  0.0 406.5 jit_solution(16740434606799057168)
XLA Ops:
  7.2 1.6 pad_maximum_fusion
  11.3 1.2 fusion.25
  12.6 1.3 fusion.27
  14.4 1.2 reshape.247
  15.9 33.0 %scatter_fusion = bf16[64,8,2048]{2,1,0:T(8,128)(2,1)S(1)} fusion(bf16[64,8,2048]{2,1,0:T(8,128)(2,1)S(1)} %broadcast_in_dim.36, s32[256]{0:T(256)S(1)} %reshape.245, bf16[256,2048]{1,0:T(8,128)(2,1)} %reshape.247), kind=kCustom, calls=%fused_computation.1 | custom fusion | bytes 3147776 | tf_op jit(solution)/shard_map/scatter | solution.py:53
  49.0 82.9 %all_to_all.30 = bf16[64,8,2048]{2,1,0:T(8,128)(2,1)} all-to-all(bf16[64,8,2048]{2,1,0:T(8,128)(2,1)S(1)} %scatter_fusion), channel_id=1, replica_groups=mesh['ep'=64,'tp'=4] {'ep'}, dimensions={0} | all-to-all | bytes 4194304 | tf_op jit(solution)/shard_map/all_to_all | solution.py:174
  132.9 5.8 %fusion.50 = (bf16[16384,1,128]{2,0,1:T(8,128)(2,1)}, bf16[16384,1,128]{2,0,1:T(8,128)(2,1)}) fusion(bf16[16384,2,128]{2,0,1:T(8,128)(2,1)} %all-gather.6.cloned.1.call-done), kind=kLoop, calls=%fused_computation.94 | loop fusion | bytes 16777216 | tf_op jit(solution)/shard_map/split | solution.py:86
  138.7 14.8 %reshape.263 = bf16[16,1024,1,2,64]{4,3,1,0,2:T(2,128)(2,1)} reshape(bf16[16384,1,128]{2,0,1:T(8,128)(2,1)} %get-tuple-element.216) | data formatting | bytes 8388608 | tf_op jit(solution)/shard_map/reshape | solution.py:98
  153.5 20.2 %copy.37 = bf16[16,1024,1,2,64]{1,4,3,2,0:T(8,128)(2,1)} copy(bf16[16,1024,1,2,64]{4,3,1,0,2:T(2,128)(2,1)} %reshape.263) | data formatting | bytes 8388608
  173.7 6.4 %copy.39 = bf16[16,1024,1,128]{1,3,2,0:T(8,128)(2,1)} copy(bf16[16,1024,1,128]{3,1,0,2:T(8,128)(2,1)} %bitcast.160) | data formatting | bytes 8388608
  180.2 25.8 %while.15 = (s32[]{:T(128)}, f32[256,1,2,2]{0,2,3,1:T(2,128)S(1)}, f32[256,1,2,2]{0,2,3,1:T(2,128)S(1)}, f32[256,1,2,2,128]{0,4,3,2,1:T(8,128)S(1)}, s32[16]{0:T...) while((s32[]{:T(128)}, f32[256,1,2,2]{0,2,3,1:T(2,128)S(1)}, ...), condition=%wide.region_5.6_spmd.clone, body=%wide.region_0.5_spmd.clone.sunk | while | flops 411570432 | bytes 15156503 | solution.py:133
  181.5 5.3 %conditional.3 = ((f32[256,1,2,2]{0,2,3,1:T(2,128)S(1)}, f32[256,1,2,2]{0,2,3,1:T(2,128)S(1)}, f32[256,1,2,2,128]{0,4,3,2,1:T(8,128)S(1)})) conditional(s32[]{:T(128)} %convert_element_type.131, (f32[256,1,2,2]{0,2,3,1:T(2,128)S(1)}, f32[256,1,2,2]{0,2,3,1:T(2,128)S(1)}, f32[256,1,2,2,128]{0,4,3,2,1:T(8,128)S(1)}) %tuple.49, (s32[]{:T(128)}, ...), branch_computations={%region_1.1_spmd, %region_2.4_spmd} | conditional | flops 411570432 | bytes 15155240 | solution.py:131
  182.4 1.8 fusion.4
  185.2 1.5 fusion.11
  206.0 11.3 %all-gather.8.cloned.1.call-done = bf16[256,8,2048]{2,1,0:T(8,128)(2,1)} async-done(((bf16[64,8,2048]{2,1,0:T(8,128)(2,1)}), bf16[256,8,2048]{2,1,0:T(8,128)(2,1)}) %all-gather.8.cloned.1.call-update) | async-done | bytes 8388624 | tf_op jit(solution)/shard_map/all_gather | solution.py:31
  217.4 5.9 %fusion.28 = f32[4,512,256]{2,1,0:T(8,128)S(1)} fusion(bf16[4,512,2048]{2,1,0:T(8,128)(2,1)} %bitcast.170, bf16[1,2048,256]{2,1,0:T(8,128)(2,1)S(1)} %copy-done), kind=kOutput, calls=%fused_computation.47 | convolution fusion | flops 2147483648 | bytes 11534336 | tf_op jit(solution)/shard_map/vmap()/dot_general | solution.py:162
  223.4 3.6 fusion.24
  227.0 4.0 all-to-all-start.2
  231.3 2.8 convolution_convert_fusion.4
  234.1 22.1 %all-to-all-done.2 = bf16[4,64,8,256]{3,2,1,0:T(8,128)(2,1)S(1)} async-done(((bf16[4,64,8,256]{3,2,1,0:T(8,128)(2,1)}), bf16[4,64,8,256]{3,2,1,0:T(8,128)(2,1)S(1)}, u32[]{:S(2)}, u32[]{:S(2)}) %all-to-all-start.2) | async-done | bytes 1048608 | tf_op jit(solution)/shard_map/all_to_all | solution.py:180
  256.1 3.7 all-to-all-start
  259.9 1.4 copy.65
  261.4 29.4 %all-gather.10.cloned.1.call-done = bf16[1,1024,2048]{2,1,0:T(8,128)(2,1)} async-done(((bf16[1,256,2048]{2,1,0:T(8,128)(2,1)}), bf16[1,1024,2048]{2,1,0:T(8,128)(2,1)}) %all-gather.10.cloned.1.call-update) | async-done | bytes 4194320 | tf_op jit(solution)/shard_map/all_gather | solution.py:181
  290.9 2.1 convolution_convert_fusion
  293.0 1.9 convolution_convert_fusion.1
  295.7 2.6 fusion.23
  299.3 37.9 %all-to-all-start.3 = ((bf16[1,64,8,2048]{3,2,0,1:T(8,128)(2,1)}), bf16[1,64,8,2048]{3,2,0,1:T(8,128)(2,1)S(1)}, u32[]{:S(2)}, u32[]{:S(2)}) async-start(bf16[1,64,8,2048]{3,2,0,1:T(8,128)(2,1)} %fusion.23), calls=%async_computation.3 | async-start | bytes 4194304 | tf_op jit(solution)/shard_map/all_to_all | solution.py:192
  338.1 2.2 reduce_sum.60
  340.3 48.1 %all-to-all-done.3 = bf16[1,64,8,2048]{3,2,0,1:T(8,128)(2,1)S(1)} async-done(((bf16[1,64,8,2048]{3,2,0,1:T(8,128)(2,1)}), bf16[1,64,8,2048]{3,2,0,1:T(8,128)(2,1)S(1)}, u32[]{:S(2)}, u32[]{:S(2)}) %all-to-all-start.3) | async-done | bytes 2097184 | tf_op jit(solution)/shard_map/all_to_all | solution.py:192
  388.4 5.2 %gather_fusion = bf16[256,2048]{1,0:T(8,128)(2,1)} fusion(bf16[64,8,2048]{2,1,0:T(8,128)(2,1)S(1)} %bitcast.159, s32[256]{0:T(256)S(1)} %reshape.239), kind=kCustom, calls=%fused_computation | custom fusion | bytes 2099200 | tf_op jit(solution)/shard_map/gather | solution.py:193
  393.7 2.4 reshape.258
  396.0 3.9 multiply_reduce_fusion
  (113 shorter events, 19.2 us)
Async XLA Ops:
  7.2 210.2 %copy-start = (bf16[1,2048,256]{2,1,0:T(8,128)(2,1)S(1)}, bf16[1,2048,256]{2,1,0:T(8,128)(2,1)}, u32[]{:S(2)}) copy-start(bf16[1,2048,256]{2,1,0:T(8,128)(2,1)} %param.28) | copy-start | bytes 3145732
  7.2 125.8 %all-gather.6.cloned.1.call-start = ((), (), s32[]{:S(2)}) async-start(), calls=%async_computation.4 | async-start | bytes 8519680 | tf_op jit(solution)/shard_map/all_gather | solution.py:87
  8.9 208.5 %all-gather.8.cloned.1.call-start = ((), (), s32[]{:S(2)}) async-start(), calls=%async_computation.5 | async-start | bytes 10485760 | tf_op jit(solution)/shard_map/all_gather | solution.py:31
  48.9 83.8 %copy-start.3 = (bf16[256,2,128]{2,1,0:T(2,128)(2,1)S(1)}, bf16[256,2,128]{2,1,0:T(2,128)(2,1)}, u32[]{:S(2)}) copy-start(bf16[256,2,128]{2,1,0:T(2,128)(2,1)} %param.17) | copy-start | bytes 393220
  49.0 83.9 %copy-start.4 = (f32[2]{0:T(128)S(1)}, f32[2]{0:T(128)}, u32[]{:S(2)}) copy-start(f32[2]{0:T(128)} %param.20) | copy-start | bytes 28
  49.0 83.9 %copy-start.5 = (f32[128]{0:T(128)S(1)}, f32[128]{0:T(128)}, u32[]{:S(2)}) copy-start(f32[128]{0:T(128)} %param.21) | copy-start | bytes 1540
  131.9 158.9 %all-gather.10.cloned.1.call-start = ((), (), s32[]{:S(2)}) async-start(), calls=%async_computation.6 | async-start | bytes 5242880 | tf_op jit(solution)/shard_map/all_gather | solution.py:181
  217.4 5.9 %copy-start.6 = (bf16[256,8,2048]{2,1,0:T(8,128)(2,1)S(1)}, bf16[256,8,2048]{2,1,0:T(8,128)(2,1)}, u32[]{:S(2)}) copy-start(bf16[256,8,2048]{2,1,0:T(8,128)(2,1)} %all-gather.8.cloned.1.call-done) | copy-start | bytes 25165828
  217.4 6.0 %copy-start.7 = (bf16[1,2048,256]{2,1,0:T(8,128)(2,1)S(1)}, bf16[1,2048,256]{2,1,0:T(8,128)(2,1)}, u32[]{:S(2)}) copy-start(bf16[1,2048,256]{2,1,0:T(8,128)(2,1)} %param.27) | copy-start | bytes 3145732
  227.0 29.1 %all-to-all-start.2 = ((bf16[4,64,8,256]{3,2,1,0:T(8,128)(2,1)}), bf16[4,64,8,256]{3,2,1,0:T(8,128)(2,1)S(1)}, u32[]{:S(2)}, u32[]{:S(2)}) async-start(bf16[4,64,8,256]{3,2,1,0:T(8,128)(2,1)} %fusion.24), calls=%async_computation.2 | async-start | bytes 2097152 | tf_op jit(solution)/shard_map/all_to_all | solution.py:180
  256.1 42.1 %all-to-all-start = ((bf16[4,64,2048]{2,1,0:T(8,128)(2,1)}), bf16[4,64,2048]{2,1,0:T(8,128)(2,1)S(1)}, u32[]{:S(2)}, u32[]{:S(2)}) async-start(bf16[4,64,2048]{2,1,0:T(8,128)(2,1)} %bitcast.26), calls=%async_computation | async-start | bytes 2097152 | tf_op jit(solution)/shard_map/all_to_all | solution.py:17
  290.9 4.0 copy-start.1
  298.3 1.0 copy-start.2
  299.3 89.2 %all-to-all-start.3 = ((bf16[1,64,8,2048]{3,2,0,1:T(8,128)(2,1)}), bf16[1,64,8,2048]{3,2,0,1:T(8,128)(2,1)S(1)}, u32[]{:S(2)}, u32[]{:S(2)}) async-start(bf16[1,64,8,2048]{3,2,0,1:T(8,128)(2,1)} %fusion.23), calls=%async_computation.3 | async-start | bytes 4194304 | tf_op jit(solution)/shard_map/all_to_all | solution.py:192
Sparse Core Ops, SparseCore 0:
  11.4 118.0 all-gather.5
  132.1 85.2 all-gather.7
  219.2 71.6 all-gather.9
